TPU v7x, 512 devices: a 4x2x32 block of a 4x8x32 slice. The times are simulated.
512 devices in a mesh: grp: 2 (over y), fs: 32 (over z), tp: 8 (over x, core).
Axes of the slice: x: 4, y: 2, z: 32, core: 2. Of those that a mesh axis runs over, the one named last changes fastest.
The devices are a block of a 4x8x32 slice.
Arguments:
- tokens: bfloat16 [24576, 2048], P(('grp', 'fs'), 'tp'), parts along dimension 0, may hold values from -6 to 6
- norm_gain: float32 [2048], P('fs'), may hold values from 0.1 to 1.9
- gate_weight: float32 [32, 2048, 1024], P(None, 'fs', 'tp'), may hold values from -0.125 to 0.125
- up_weight: float32 [32, 2048, 1024], P(None, 'fs', 'tp'), may hold values from -0.125 to 0.125
- down_weight: float32 [32, 2048, 1024], P(None, 'fs', 'tp'), may hold values from -0.5 to 0.5
- expert_ids: int32 [24576, 2], P(('grp', 'fs')), parts along dimension 0, may hold values from 0 to 31, as said below
- group_logits: float32 [24576, 2], P(('grp', 'fs')), parts along dimension 0, may hold values from -2.5 to 2.5
- pair_logits: float32 [24576, 2], P(('grp', 'fs')), parts along dimension 0, may hold values from -2.5 to 2.5
Outputs:
- mixed: bfloat16 [24576, 2048], P(('grp', 'fs'), 'tp'), parts along dimension 0
- gate_out: bfloat16 [64, 2048, 1024], P(('grp', 'fs'), None, 'tp'), parts along dimension 0
- up_out: bfloat16 [64, 2048, 1024], P(('grp', 'fs'), None, 'tp'), parts along dimension 0
- down_out: bfloat16 [64, 2048, 1024], P(('grp', 'fs'), None, 'tp'), parts along dimension 0
There are 2 independent parts, one for each index of `grp`. A program takes and returns all parts, laid end to end along the dimension named above; an argument that names none is the same for every part. Nothing has to cross between parts.
Inputs may be any that keep to these rules, and one draw needn't show every extreme that they name: `expert_ids`: each row names two different experts of one group: both ids lie in the same run of 16 consecutive ids.
All inputs are finite; a program needn't handle non-finite values.
Results may differ from a plain program's by a relative error of at most 0.015.
Values may be sent and summed in bfloat16 or wider, within the bound.
A program may use at most 64 MiB of HBM per device.

v0:
```python
import jax
import jax.numpy as jnp
from jax import lax
from jax.sharding import PartitionSpec as P


def in_one_piece(arrays, axis, split_dim, concat_dim, along):
    widths = [a.shape[along] for a in arrays]
    both = jnp.concatenate(arrays, axis=along)
    result = lax.all_to_all(both, axis, split_axis=split_dim, concat_axis=concat_dim, tiled=True)
    return tuple(jnp.split(result, [sum(widths[:k]) for k in range(1, len(widths))], axis=along))


def routing(block_ids, experts, capacity):
    entries = block_ids.reshape(-1)
    onehot = (entries[:, None] == jnp.arange(experts, dtype=jnp.int32)[None, :]).astype(jnp.int32)
    before = jnp.cumsum(onehot, axis=0) - onehot
    entry_rank = jnp.sum(before * onehot, axis=1)
    kept = entry_rank < capacity
    slot_index = jnp.where(kept, entries * capacity + entry_rank, experts * capacity)
    return (slot_index, kept)


def fill_slots(block_rows, slot_index, experts, capacity):
    entry_count = slot_index.shape[0]
    source_row = jnp.arange(entry_count, dtype=jnp.int32) // 2
    slot_row = jnp.zeros((experts * capacity + 1,), jnp.int32).at[slot_index].set(source_row)
    filled = jnp.zeros((experts * capacity + 1,), jnp.float32).at[slot_index].set(1.0)
    chosen = block_rows[slot_row[: experts * capacity]]
    return chosen * filled[: experts * capacity, None].astype(block_rows.dtype)


def route_weights(block_ids, group_logits, pair_logits, kept, exp_group):
    group_pick = block_ids[:, 0] // exp_group
    group_exp = jnp.exp(group_logits)
    columns = jnp.arange(group_logits.shape[1], dtype=jnp.int32)
    chosen = jnp.sum(jnp.where(columns[None, :] == group_pick[:, None], group_exp, 0.0), axis=1)
    chosen = chosen / jnp.sum(group_exp, axis=1)
    pair_exp = jnp.exp(pair_logits)
    weights = pair_exp / jnp.sum(pair_exp, axis=1, keepdims=True) * chosen[:, None]
    return weights * kept.reshape(-1, 2).astype(weights.dtype)


def body(
    tokens, norm_gain, gate_weight, up_weight, down_weight, expert_ids, group_logits, pair_logits
):
    experts = gate_weight.shape[0]
    tok_rows = tokens.shape[0]
    capacity = 5 * tok_rows * 2 // (4 * experts)
    shard_count = lax.axis_size("fs")
    scaled = norm_gain[None, :, None]
    gate_cast = (scaled * gate_weight).astype(jnp.bfloat16)
    up_cast = (scaled * up_weight).astype(jnp.bfloat16)
    down_cast = down_weight.astype(jnp.bfloat16)
    slot_index, kept = routing(expert_ids, experts, capacity)
    weights = route_weights(
        expert_ids, group_logits, pair_logits, kept, experts // group_logits.shape[1]
    )
    gate_here, up_here, down_here = in_one_piece((gate_cast, up_cast, down_cast), "fs", 0, 1, 2)
    gate_local = gate_here[0]
    up_local = up_here[0]
    outgoing = fill_slots(tokens, slot_index, experts, capacity)
    arrived = lax.all_to_all(
        outgoing.reshape(experts, capacity, -1), "fs", split_axis=0, concat_axis=0, tiled=True
    )
    arrived = arrived.reshape(shard_count * capacity, -1)
    piece = lax.all_gather(arrived, "tp", axis=1, tiled=True)
    gate_pre = jnp.dot(piece, gate_local, preferred_element_type=jnp.float32)
    up_pre = jnp.dot(piece, up_local, preferred_element_type=jnp.float32)
    hidden = (jax.nn.silu(gate_pre) * up_pre).astype(jnp.bfloat16)
    terms = lax.dot_general(
        hidden, down_here[0], (((1,), (1,)), ((), ())), preferred_element_type=jnp.float32
    )
    expert_rows = lax.psum_scatter(
        terms.astype(jnp.bfloat16), "tp", scatter_dimension=1, tiled=True
    )
    returned = lax.all_to_all(
        expert_rows.reshape(shard_count, capacity, -1),
        "fs",
        split_axis=0,
        concat_axis=0,
        tiled=True,
    )
    returned = returned.reshape(experts * capacity, -1)
    picked = returned[jnp.clip(slot_index, 0, experts * capacity - 1)].astype(jnp.float32)
    picked = picked.reshape(tok_rows, 2, -1)
    mixed = jnp.sum(picked * weights[:, :, None], axis=1).astype(jnp.bfloat16)
    return (mixed, gate_here, up_here, down_here)


def solution(mesh):
    placed = (
        P(("grp", "fs"), "tp"),
        P("fs"),
        P(None, "fs", "tp"),
        P(None, "fs", "tp"),
        P(None, "fs", "tp"),
        P(("grp", "fs"), None),
        P(("grp", "fs"), None),
        P(("grp", "fs"), None),
    )
    return jax.shard_map(
        body,
        mesh=mesh,
        in_specs=placed,
        out_specs=(
            P(("grp", "fs"), "tp"),
            P(("grp", "fs"), None, "tp"),
            P(("grp", "fs"), None, "tp"),
            P(("grp", "fs"), None, "tp"),
        ),
        check_vma=False,
    )
```

profile of v0, /device:TPU:33, one launch (start us, length us, event | category | flops | bytes accessed | tf_op | source)
XLA Modules:
  0.0 432.5 jit_solution(1233582038870439962)
XLA Ops:
  7.2 0.9 copy.25
  8.1 0.1 eq.44
  8.2 0.1 eq.40
  8.4 0.7 broadcast_multiply_fusion.1
  9.1 1.7 reduce-window.6
  10.8 0.3 slice_reduce_fusion
  11.1 0.1 copy.28
  11.2 0.2 mul.71
  11.6 3.4 scatter_custom_fusion
  15.0 4.1 gather_fusion
  19.1 0.1 gather.9
  19.2 3.4 scatter_custom_fusion.1
  22.7 1.0 broadcast_multiply_fusion
  23.7 46.3 %all-to-all-start = ((bf16[32,30,256]{2,1,0:T(8,128)(2,1)}), bf16[32,30,256]{2,1,0:T(8,128)(2,1)S(1)}, u32[]{:S(2)}, u32[]{:S(2)}) async-start(bf16[32,30,256]{2,1,0:T(8,128)(2,1)} %broadcast_multiply_fusion), calls=%async_computation | async-start | bytes 1048576 | tf_op jit(solution)/shard_map/all_to_all | solution.py:63
  70.2 1.5 multiply_convert_fusion.1
  71.7 1.4 pad_maximum_fusion
  73.1 60.8 %all-to-all-done = bf16[32,30,256]{2,1,0:T(8,128)(2,1)S(1)} async-done(((bf16[32,30,256]{2,1,0:T(8,128)(2,1)}), bf16[32,30,256]{2,1,0:T(8,128)(2,1)S(1)}, u32[]{:S(2)}, u32[]{:S(2)}) %all-to-all-start) | async-done | bytes 491552 | tf_op jit(solution)/shard_map/all_to_all | solution.py:63
  133.9 4.9 %all-to-all-start.1 = ((bf16[32,64,384]{2,1,0:T(8,128)(2,1)}), bf16[32,64,384]{2,1,0:T(8,128)(2,1)S(1)}, u32[]{:S(2)}, u32[]{:S(2)}) async-start(bf16[32,64,384]{2,1,0:T(8,128)(2,1)} %pad_maximum_fusion), calls=%async_computation.1 | async-start | bytes 3145728 | tf_op jit(solution)/shard_map/all_to_all | solution.py:10
  138.9 1.0 reshape.120
  140.0 146.3 %all-to-all-done.1 = bf16[32,64,384]{2,1,0:T(8,128)(2,1)S(1)} async-done(((bf16[32,64,384]{2,1,0:T(8,128)(2,1)}), bf16[32,64,384]{2,1,0:T(8,128)(2,1)S(1)}, u32[]{:S(2)}, u32[]{:S(2)}) %all-to-all-start.1) | async-done | bytes 1572896 | tf_op jit(solution)/shard_map/all_to_all | solution.py:10
  286.3 0.3 fusion.28
  286.7 3.8 fusion.4
  290.5 8.1 %convolution_convert_fusion = bf16[960,2048]{1,0:T(8,128)(2,1)} fusion(bf16[960,2048]{1,0:T(8,128)(2,1)} %all-gather.2.cloned.1.call-done, bf16[1,2048,128]{2,1,0:T(8,128)(2,1)S(1)} %get-tuple-element.9, bf16[1,2048,128]{2,1,0:T(8,128)(2,1)S(1)} %get-tuple-element.10, f32[960,128]{1,0:T(8,128)S(1)} %fusion.4), kind=kOutput, calls=%fused_computation.4 | convolution fusion | flops 1009336320 | bytes 9404416 | tf_op jit(solution)/shard_map/dot_general | solution.py:71
  298.7 42.2 %reduce-scatter.2.cloned.1.call-done = bf16[960,256]{1,0:T(8,128)(2,1)} async-done(((bf16[960,2048]{1,0:T(8,128)(2,1)}), bf16[960,256]{1,0:T(8,128)(2,1)}) %reduce-scatter.2.cloned.1.call-update) | async-done | bytes 491536 | tf_op jit(solution)/shard_map/reduce_scatter | solution.py:74
  340.9 2.0 reshape.121
  342.9 21.1 %all-to-all-start.2 = ((bf16[32,30,256]{2,1,0:T(8,128)(2,1)}), bf16[32,30,256]{2,1,0:T(8,128)(2,1)S(1)}, u32[]{:S(2)}, u32[]{:S(2)}) async-start(bf16[32,30,256]{2,1,0:T(8,128)(2,1)} %reshape.121), calls=%async_computation.3 | async-start | bytes 1048576 | tf_op jit(solution)/shard_map/all_to_all | solution.py:77
  364.0 0.2 lt.53
  364.5 0.1 copy.30
  364.6 56.1 %all-to-all-done.2 = bf16[32,30,256]{2,1,0:T(8,128)(2,1)S(1)} async-done(((bf16[32,30,256]{2,1,0:T(8,128)(2,1)}), bf16[32,30,256]{2,1,0:T(8,128)(2,1)S(1)}, u32[]{:S(2)}, u32[]{:S(2)}) %all-to-all-start.2) | async-done | bytes 491552 | tf_op jit(solution)/shard_map/all_to_all | solution.py:77
  420.9 2.7 gather_fusion.1
  423.6 0.4 reshape.123
  423.9 1.7 multiply_reduce_fusion
  (45 shorter events, 1.1 us)
Async XLA Ops:
  7.2 7.8 %copy-start = (bf16[384,256]{1,0:T(8,128)(2,1)S(1)}, bf16[384,256]{1,0:T(8,128)(2,1)}, u32[]{:S(2)}) copy-start(bf16[384,256]{1,0:T(8,128)(2,1)} %param.8) | copy-start | bytes 589828
  15.0 55.1 %copy-start.4 = (f32[32,64,128]{2,1,0:T(8,128)S(1)}, f32[32,64,128]{2,1,0:T(8,128)}, u32[]{:S(2)}) copy-start(f32[32,64,128]{2,1,0:T(8,128)} %param.12) | copy-start | bytes 3145732
  19.0 51.1 %copy-start.9 = (f32[64]{0:T(128)S(1)}, f32[64]{0:T(128)}, u32[]{:S(2)}) copy-start(f32[64]{0:T(128)} %param.9) | copy-start | bytes 772
  19.2 51.0 %copy-start.5 = (f32[32,64,128]{2,1,0:T(8,128)S(1)}, f32[32,64,128]{2,1,0:T(8,128)}, u32[]{:S(2)}) copy-start(f32[32,64,128]{2,1,0:T(8,128)} %param.10) | copy-start | bytes 3145732
  23.7 110.2 %all-to-all-start = ((bf16[32,30,256]{2,1,0:T(8,128)(2,1)}), bf16[32,30,256]{2,1,0:T(8,128)(2,1)S(1)}, u32[]{:S(2)}, u32[]{:S(2)}) async-start(bf16[32,30,256]{2,1,0:T(8,128)(2,1)} %broadcast_multiply_fusion), calls=%async_computation | async-start | bytes 1048576 | tf_op jit(solution)/shard_map/all_to_all | solution.py:63
  133.9 152.4 %all-to-all-start.1 = ((bf16[32,64,384]{2,1,0:T(8,128)(2,1)}), bf16[32,64,384]{2,1,0:T(8,128)(2,1)S(1)}, u32[]{:S(2)}, u32[]{:S(2)}) async-start(bf16[32,64,384]{2,1,0:T(8,128)(2,1)} %pad_maximum_fusion), calls=%async_computation.1 | async-start | bytes 3145728 | tf_op jit(solution)/shard_map/all_to_all | solution.py:10
  138.8 147.8 %all-gather.2.cloned.1.call-start = ((), (), s32[]{:S(2)}) async-start(), calls=%async_computation.4 | async-start | bytes 4423680 | tf_op jit(solution)/shard_map/all_gather | solution.py:67
  139.9 201.0 %reduce-scatter.2.cloned.1.call-start = ((), (), s32[]{:S(2)}) async-start(), calls=%async_computation.5 | async-start | bytes 4423680 | tf_op jit(solution)/shard_map/reduce_scatter | solution.py:74
  286.6 12.0 %copy-start.1 = (bf16[1,2048,128]{2,1,0:T(8,128)(2,1)}, bf16[1,2048,128]{2,1,0:T(8,128)(2,1)S(1)}, u32[]{:S(2)}) copy-start(bf16[1,2048,128]{2,1,0:T(8,128)(2,1)S(1)} %get-tuple-element.8) | copy-start | bytes 1572868
  286.6 12.0 %copy-start.2 = (bf16[1,2048,128]{2,1,0:T(8,128)(2,1)}, bf16[1,2048,128]{2,1,0:T(8,128)(2,1)S(1)}, u32[]{:S(2)}) copy-start(bf16[1,2048,128]{2,1,0:T(8,128)(2,1)S(1)} %get-tuple-element.9) | copy-start | bytes 1572868
  286.6 12.0 %copy-start.3 = (bf16[1,2048,128]{2,1,0:T(8,128)(2,1)}, bf16[1,2048,128]{2,1,0:T(8,128)(2,1)S(1)}, u32[]{:S(2)}) copy-start(bf16[1,2048,128]{2,1,0:T(8,128)(2,1)S(1)} %get-tuple-element.10) | copy-start | bytes 1572868
  298.6 65.7 %copy-start.6 = (s32[384,2]{0,1:T(2,128)S(1)}, s32[384,2]{0,1:T(2,128)}, u32[]{:S(2)}) copy-start(s32[384,2]{0,1:T(2,128)} %param.13) | copy-start | bytes 9220
  298.6 65.7 %copy-start.8 = (f32[384,2]{0,1:T(2,128)S(1)}, f32[384,2]{0,1:T(2,128)}, u32[]{:S(2)}) copy-start(f32[384,2]{0,1:T(2,128)} %param.14) | copy-start | bytes 9220
  298.6 65.8 %copy-start.7 = (f32[384,2]{0,1:T(2,128)S(1)}, f32[384,2]{0,1:T(2,128)}, u32[]{:S(2)}) copy-start(f32[384,2]{0,1:T(2,128)} %param.15) | copy-start | bytes 9220
  342.9 77.9 %all-to-all-start.2 = ((bf16[32,30,256]{2,1,0:T(8,128)(2,1)}), bf16[32,30,256]{2,1,0:T(8,128)(2,1)S(1)}, u32[]{:S(2)}, u32[]{:S(2)}) async-start(bf16[32,30,256]{2,1,0:T(8,128)(2,1)} %reshape.121), calls=%async_computation.3 | async-start | bytes 1048576 | tf_op jit(solution)/shard_map/all_to_all | solution.py:77
Sparse Core Ops, SparseCore 0:
  141.8 52.6 all-gather.1
  298.8 42.0 reduce-scatter.1
where the time goes:
time: 440 us; the launch traced here: 433 us
  waiting for transfers between devices  306 us (70%)
  starting transfers between devices  72.4 us (16%)
  local copies, waits for them, and re-layouts  19.6 us (4%)
  between operations  14.4 us (3%)
  matrix products  11.9 us (3%)
  other arithmetic  8.48 us (2%)
    all_to_all x1, waiting for transfers between devices, in_one_piece(): lax.all_to_all(both, axis, split_axis=split_dim, concat_axis=concat_dim,...  146 us
    all_to_all x1, waiting for transfers between devices, body(): lax.all_to_all(outgoing.reshape(experts, capacity, -1), 'fs', split_axis=...  60.8 us
    all_to_all x1, waiting for transfers between devices, body(): lax.all_to_all(expert_rows.reshape(shard_count, capacity, -1), 'fs', spli...  56.1 us
    all_to_all x1, starting transfers between devices, body(): lax.all_to_all(outgoing.reshape(experts, capacity, -1), 'fs', split_axis=...  46.3 us
    reduce_scatter x1, waiting for transfers between devices, body(): lax.psum_scatter(terms.astype(jnp.bfloat16), 'tp', scatter_dimension=1, t...  42.2 us
    all_to_all x1, starting transfers between devices, body(): lax.all_to_all(expert_rows.reshape(shard_count, capacity, -1), 'fs', spli...  21.1 us
  transfers between devices with their start and end apart: 5, of which 4 were waited for; matrix products, arithmetic and copies ran while one was open for 1% of the time, Pallas kernels for 0%

commit v1 on v0

v1 whole, which is shorter than its diff:
```python
import functools

import jax
import jax.numpy as jnp
from jax import lax
from jax.experimental import pallas as pl
from jax.experimental.pallas import tpu as pltpu
from jax.sharding import PartitionSpec as P

MESH = pl.DeviceIdType.MESH
BF = jnp.bfloat16
F32 = jnp.float32


def kernel(
    cfg, tok_hbm, gain, gate_hbm, up_hbm, down_hbm, ids, glog, plog,
    mixed, gate_o, up_o, down_o,
    wf, wstage, wbuf, wother, gu, dn, tokv, outs, trecv, piece, part, rsbuf, res, ret, onehot, cols,
    lsem, osem, ws, wr, ts, tr, rs, rr, ys, yr, ds, dr, ags, agr, rss, rsr,
):
    n, groups, tps, cap, slots, nq, ck = cfg
    half = n // 2
    tok_rows, width = tokv.shape
    me, grp, tp = lax.axis_index("fs"), lax.axis_index("grp"), lax.axis_index("tp")
    core = lax.rem(tp, 2)
    partner = tp + 1 - 2 * core

    loads = [
        pltpu.make_async_copy(src.at[:, grp], wf.at[i], lsem.at[i])
        for i, src in enumerate((gate_hbm, up_hbm, down_hbm))
    ]
    for load in loads:
        load.start()
    tok_load = pltpu.make_async_copy(tok_hbm, tokv, lsem.at[3])
    tok_load.start()

    barrier = pltpu.get_barrier_semaphore()

    def greet(axis, here, size):
        def one(o, c):
            pl.semaphore_signal(
                barrier, inc=1, device_id={axis: lax.rem(here + o, size)}, device_id_type=MESH
            )
            return c

        lax.fori_loop(1, size, one, 0)

    greet("fs", me, n)
    greet("tp", tp, tps)
    greet("grp", grp, groups)

    for i, load in enumerate(loads):
        load.wait()
        if i < 2:
            wstage[:, i] = (wf[i] * gain[grp][None]).astype(BF)
        else:
            wstage[:, i] = wf[i].astype(BF)
        wbuf[i, me, grp] = wstage[me, i]

    pl.semaphore_wait(barrier, n - 1 + tps - 1 + groups - 1)

    def delta_of(h, k):
        return half - 1 - k if h == 0 else half + k

    def to(h, k):
        return lax.rem(me + delta_of(h, k), n)

    def back(h, k):
        return lax.rem(me + n - delta_of(h, k), n)

    def every(fn, lo=0, hi=half):
        def one(k, c):
            fn(0, k)
            fn(1, k)
            return c

        last = min(hi, half - 1)
        lax.fori_loop(lo, last, one, 0)
        if hi == half:
            fn(1, half - 1)

    def w_copy(h, k, dst, src):
        return pltpu.make_async_remote_copy(
            src_ref=wstage.at[dst], dst_ref=wbuf.at[:, src, grp],
            send_sem=ws.at[h, k], recv_sem=wr.at[h, k],
            device_id={"fs": dst}, device_id_type=MESH,
        )

    def t_copy(h, k, dst):
        return pltpu.make_async_remote_copy(
            src_ref=outs.at[dst], dst_ref=trecv.at[h, k],
            send_sem=ts.at[h, k], recv_sem=tr.at[h, k],
            device_id={"fs": dst}, device_id_type=MESH,
        )

    def r_copy(h, k, dst, src):
        return pltpu.make_async_remote_copy(
            src_ref=res.at[h, k], dst_ref=ret.at[src],
            send_sem=rs.at[h, k], recv_sem=rr.at[h, k],
            device_id={"fs": dst}, device_id_type=MESH,
        )

    every(lambda h, k: w_copy(h, k, to(h, k), me).start())

    exp_group = n // glog.shape[0]
    first, second = ids[0:1, :], ids[1:2, :]
    e_iota = lax.broadcasted_iota(jnp.int32, (n, tok_rows), 0)
    is0, is1 = e_iota == first, e_iota == second
    count = (is0 | is1).astype(F32).astype(BF)
    earlier = (
        lax.broadcasted_iota(jnp.int32, (tok_rows, tok_rows), 0)
        < lax.broadcasted_iota(jnp.int32, (tok_rows, tok_rows), 1)
    ).astype(F32).astype(BF)
    before = jnp.dot(count, earlier, preferred_element_type=F32)
    rank0 = jnp.sum(jnp.where(is0, before, 0.0), axis=0, keepdims=True)
    rank1 = jnp.sum(jnp.where(is1, before, 0.0), axis=0, keepdims=True)
    keep0, keep1 = rank0 < cap, rank1 < cap
    slot0 = jnp.where(keep0, first.astype(F32) * slots + rank0, -1.0)
    slot1 = jnp.where(keep1, second.astype(F32) * slots + rank1, -1.0)

    group_exp = [jnp.exp(glog[g : g + 1, :]) for g in range(glog.shape[0])]
    chosen, total = jnp.zeros_like(slot0), jnp.zeros_like(slot0)
    for g, value in enumerate(group_exp):
        mine = (first >= g * exp_group) & (first < (g + 1) * exp_group)
        chosen += jnp.where(mine, value, 0.0)
        total += value
    chosen = chosen / total
    pair0, pair1 = jnp.exp(plog[0:1, :]), jnp.exp(plog[1:2, :])
    weight0 = jnp.where(keep0, pair0 / (pair0 + pair1) * chosen, 0.0)
    weight1 = jnp.where(keep1, pair1 / (pair0 + pair1) * chosen, 0.0)

    tok_load.wait()
    tokens = tokv[...]
    slot0i, slot1i = slot0.astype(jnp.int32), slot1.astype(jnp.int32)
    build = 4 * slots
    s_iota = lax.broadcasted_iota(jnp.int32, (build, tok_rows), 0)

    def fill(b, c):
        at = s_iota + b * build
        pick = ((at == slot0i) | (at == slot1i)).astype(F32).astype(BF)
        rows = jnp.dot(pick, tokens, preferred_element_type=F32).astype(BF)
        outs[pl.ds(b * 4, 4)] = rows.reshape(4, slots, width)
        return c

    lax.fori_loop(0, n // 4, fill, 0)

    every(lambda h, k: t_copy(h, k, to(h, k)).start())
    trecv[0, half - 1] = outs[me]

    lines = lax.broadcasted_iota(jnp.int32, (128, tok_rows), 0)
    packed = jnp.zeros((128, tok_rows), F32)
    for i, row in enumerate((slot0, slot1, weight0, weight1)):
        packed = jnp.where(lines == i, row, packed)
    cols[...] = packed.T
    l_iota = lax.broadcasted_iota(jnp.int32, (tok_rows, n * slots), 1)
    for i in range(2):
        onehot[i] = (l_iota == cols[:, i : i + 1].astype(jnp.int32)).astype(F32).astype(BF)

    every(lambda h, k: w_copy(h, k, to(h, k), back(h, k)).wait_recv())

    def y_copy(o, there, whose):
        return pltpu.make_async_remote_copy(
            src_ref=wbuf.at[:, :, grp], dst_ref=wbuf.at[:, :, whose],
            send_sem=ys.at[o], recv_sem=yr.at[o],
            device_id={"grp": there}, device_id_type=MESH,
        )

    for o in range(1, groups):
        y_copy(o, lax.rem(grp + o, groups), grp).start()
    for o in range(1, groups):
        y_copy(o, lax.rem(grp + o, groups), lax.rem(grp + groups - o, groups)).wait_recv()

    exchange = pltpu.make_async_remote_copy(
        src_ref=wbuf, dst_ref=wother, send_sem=ds, recv_sem=dr,
        device_id={"tp": partner}, device_id_type=MESH,
    )
    exchange.start()
    stores = [
        pltpu.make_async_copy(wbuf.at[i], dst, osem.at[i])
        for i, dst in enumerate((gate_o, up_o, down_o))
    ]
    for store in stores:
        store.start()

    def ag_copy(q, o, there, whose):
        h = lax.rem(there, 2)
        return pltpu.make_async_remote_copy(
            src_ref=trecv.at[h, pl.ds(q * ck, ck)], dst_ref=piece.at[q, whose],
            send_sem=ags.at[q, o], recv_sem=agr.at[q, o],
            device_id={"tp": there}, device_id_type=MESH,
        )

    def rs_copy(q, o, there, whose):
        return pltpu.make_async_remote_copy(
            src_ref=part.at[q, there], dst_ref=rsbuf.at[q, whose],
            send_sem=rss.at[q, o], recv_sem=rsr.at[q, o],
            device_id={"tp": there}, device_id_type=MESH,
        )

    def ahead(o):
        return lax.rem(tp + o, tps)

    def behind(o):
        return lax.rem(tp + tps - o, tps)

    def around(fn):
        def one(o, c):
            fn(o)
            return c

        lax.fori_loop(1, tps, one, 0)

    def gather(q):
        every(lambda h, k: t_copy(h, k, to(h, k)).wait_recv(), q * ck, (q + 1) * ck)
        around(lambda o: ag_copy(q, o, ahead(o), tp).start())
        piece[q, tp] = trecv[core, q * ck : (q + 1) * ck]

    def work(q):
        around(lambda o: ag_copy(q, o, ahead(o), behind(o)).wait_recv())
        rows = ck * slots
        acc = jnp.zeros((rows, gu.shape[1]), F32)
        for j in range(tps):
            acc += jnp.dot(
                piece[q, j].reshape(rows, width), gu[j * width : (j + 1) * width, :],
                preferred_element_type=F32,
            )
        f = gu.shape[1] // 4
        hidden = []
        for i in range(2):
            gate_v, up_v = acc[:, 2 * i * f : (2 * i + 1) * f], acc[:, (2 * i + 1) * f : (2 * i + 2) * f]
            hidden.append((gate_v / (1.0 + jnp.exp(-gate_v)) * up_v).astype(BF))
        hidden = jnp.concatenate(hidden, axis=1)
        for j in range(tps):
            term = lax.dot_general(
                hidden, dn[j * width : (j + 1) * width, :], (((1,), (1,)), ((), ())),
                preferred_element_type=F32,
            )
            part[q, j] = term.astype(BF).reshape(ck, slots, width)
        around(lambda o: rs_copy(q, o, ahead(o), tp).start())
        rsbuf[q, tp] = part[q, tp]

    def finish(q):
        around(lambda o: rs_copy(q, o, ahead(o), behind(o)).wait_recv())
        for h in range(2):
            total = rsbuf[q, h].astype(F32)
            for chip in range(1, tps // 2):
                total += rsbuf[q, 2 * chip + h].astype(F32)
            res[h, q * ck : (q + 1) * ck] = total.astype(BF)
        every(lambda h, k: r_copy(h, k, back(h, k), me).start(), q * ck, (q + 1) * ck)

    gather(0)
    exchange.wait_recv()
    f = wbuf.shape[-1]
    depth = gu.shape[0]
    for i, src in enumerate((wbuf, wother)):
        gu[:, 2 * i * f : (2 * i + 1) * f] = src[0].reshape(depth, f)
        gu[:, (2 * i + 1) * f : (2 * i + 2) * f] = src[1].reshape(depth, f)
        dn[:, i * f : (i + 1) * f] = src[2].reshape(depth, f)

    todo = []
    for q in range(nq):
        todo += [(2 * q + 0.0, gather, q), (2 * q + 1.1, work, q), (2 * q + 3.2, finish, q)]
    for _, step, q in sorted(todo, key=lambda item: item[0])[1:]:
        step(q)

    ret[me] = res[0, half - 1]
    every(lambda h, k: r_copy(h, k, back(h, k), to(h, k)).wait_recv())
    table = ret[...].reshape(n * slots, width)
    mix = jnp.zeros((tok_rows, width), F32)
    for i in range(2):
        rows = jnp.dot(onehot[i], table, preferred_element_type=F32)
        mix += rows * cols[:, 2 + i : 3 + i]
    mixed[...] = mix.astype(BF)

    for store in stores:
        store.wait()
    every(lambda h, k: w_copy(h, k, to(h, k), me).wait_send())
    every(lambda h, k: t_copy(h, k, to(h, k)).wait_send())
    every(lambda h, k: r_copy(h, k, back(h, k), me).wait_send())
    for o in range(1, groups):
        y_copy(o, lax.rem(grp + o, groups), grp).wait_send()
    exchange.wait_send()
    for q in range(nq):
        around(lambda o: ag_copy(q, o, ahead(o), tp).wait_send())
        around(lambda o: rs_copy(q, o, ahead(o), tp).wait_send())


def body(chunks, tokens, norm_gain, gate_weight, up_weight, down_weight, ids, group_logits, pair_logits):
    experts, rows, f = gate_weight.shape
    tok_rows, width = tokens.shape
    n, groups, tps = lax.axis_size("fs"), lax.axis_size("grp"), lax.axis_size("tp")
    cap = 5 * tok_rows * 2 // (4 * experts)
    slots = -(-cap // 16) * 16
    half = n // 2
    ck = half // chunks
    share = rows // groups
    depth = n * rows

    def cut(weight):
        return weight.reshape(experts, groups, share, f)

    gain = jnp.broadcast_to(norm_gain[:, None], (rows, f)).reshape(groups, share, f)
    vmem = pl.BlockSpec(memory_space=pltpu.VMEM)
    hbm = pl.BlockSpec(memory_space=pl.ANY)
    whole = jax.ShapeDtypeStruct((n, groups, share, f), BF)
    dma = pltpu.SemaphoreType.DMA
    out = pl.pallas_call(
        functools.partial(kernel, (n, groups, tps, cap, slots, chunks, ck)),
        out_shape=(jax.ShapeDtypeStruct((tok_rows, width), BF), whole, whole, whole),
        in_specs=[hbm, vmem, hbm, hbm, hbm, vmem, vmem, vmem],
        out_specs=(vmem, hbm, hbm, hbm),
        scratch_shapes=[
            pltpu.VMEM((3, n, share, f), F32),
            pltpu.VMEM((n, 3, share, f), BF),
            pltpu.VMEM((3, n, groups, share, f), BF),
            pltpu.VMEM((3, n, groups, share, f), BF),
            pltpu.VMEM((depth, 4 * f), BF),
            pltpu.VMEM((depth, 2 * f), BF),
            pltpu.VMEM((tok_rows, width), BF),
            pltpu.VMEM((n, slots, width), BF),
            pltpu.VMEM((2, half, slots, width), BF),
            pltpu.VMEM((chunks, tps, ck, slots, width), BF),
            pltpu.VMEM((chunks, tps, ck, slots, width), BF),
            pltpu.VMEM((chunks, tps, ck, slots, width), BF),
            pltpu.VMEM((2, half, slots, width), BF),
            pltpu.VMEM((n, slots, width), BF),
            pltpu.VMEM((2, tok_rows, n * slots), BF),
            pltpu.VMEM((tok_rows, 128), F32),
            dma((4,)), dma((3,)),
            dma((2, half)), dma((2, half)),
            dma((2, half)), dma((2, half)),
            dma((2, half)), dma((2, half)),
            dma((groups,)), dma((groups,)),
            dma, dma,
            dma((chunks, tps)), dma((chunks, tps)),
            dma((chunks, tps)), dma((chunks, tps)),
        ],
        compiler_params=pltpu.CompilerParams(collective_id=0, has_side_effects=True),
    )(
        tokens, gain, cut(gate_weight), cut(up_weight), cut(down_weight),
        ids.T, group_logits.T, pair_logits.T,
    )
    mixed, gate_out, up_out, down_out = out
    return (mixed,) + tuple(w.reshape(1, depth, f) for w in (gate_out, up_out, down_out))


def solution(mesh, chunks=4):
    placed = (
        P(("grp", "fs"), "tp"),
        P("fs"),
        P(None, "fs", "tp"),
        P(None, "fs", "tp"),
        P(None, "fs", "tp"),
        P(("grp", "fs"), None),
        P(("grp", "fs"), None),
        P(("grp", "fs"), None),
    )
    return jax.shard_map(
        functools.partial(body, chunks),
        mesh=mesh,
        in_specs=placed,
        out_specs=(
            P(("grp", "fs"), "tp"),
            P(("grp", "fs"), None, "tp"),
            P(("grp", "fs"), None, "tp"),
            P(("grp", "fs"), None, "tp"),
        ),
        check_vma=False,
    )
```

time: 440 us -> 239 us (0.54); the launches traced: 433 us -> 238 us
  waiting for transfers between devices: 306 us -> 0 us
  Pallas kernels: 0 us -> 231 us
  starting transfers between devices: 72.4 us -> 0 us
  between operations: 14.4 us -> 0.65 us
  local copies, waits for them, and re-layouts: 19.6 us -> 6.99 us
  matrix products: 11.9 us -> 0 us
  other arithmetic: 8.48 us -> 0 us
    all_to_all x3 -> x0, waiting for transfers between devices: 263 us -> none  [the longest x1 146 us: in_one_piece(): lax.all_to_all(both, axis, split_axis=split_dim, concat_axis=concat_dim,...]
    pallas_call x0 -> x1, Pallas kernels: none -> 231 us  [body(): pl.pallas_call(functools.partial(kernel, (n, groups, tps, cap, slots, chu...]
    all_to_all x3 -> x0, starting transfers between devices: 72.3 us -> none  [the longest x1 46.3 us: body(): lax.all_to_all(outgoing.reshape(experts, capacity, -1), 'fs', split_axis=...]
    reduce_scatter x1 -> x0, waiting for transfers between devices: 42.2 us -> none  [body(): lax.psum_scatter(terms.astype(jnp.bfloat16), 'tp', scatter_dimension=1, t...]
    dot_general x2 -> x0, matrix products: 11.9 us -> none  [the longest x1 8.1 us: body(): lax.dot_general(hidden, down_here[0], (((1,), (1,)), ((), ())), preferred...]
    gather x3 -> x0, local copies, waits for them, and re-layouts: 6.84 us -> none  [the longest x2 4.19 us: fill_slots(): chosen = block_rows[slot_row[:experts * capacity]]]
    scatter x2 -> x0, local copies, waits for them, and re-layouts: 6.76 us -> none  [the longest x1 3.38 us: fill_slots(): jnp.zeros((experts * capacity + 1,), jnp.int32).at[slot_index]]
    unnamed x21 -> x10, local copies, waits for them, and re-layouts: 0.92 us -> 6.22 us
  transfers between devices with their start and end apart: 5 -> 0, of which waited for: 4 -> 0; matrix products, arithmetic and copies ran while one was open for 1% -> 0% of each run, Pallas kernels for 0% -> 0%
where the time goes in v1:
time: 239 us; the launch traced here: 238 us
  Pallas kernels  231 us (97%)
  local copies, waits for them, and re-layouts  6.99 us (3%)
    pallas_call x1, Pallas kernels, body(): pl.pallas_call(functools.partial(kernel, (n, groups, tps, cap, slots, chu...  231 us
    unnamed x10, local copies, waits for them, and re-layouts  6.22 us

profile of v1, /device:TPU:33, one launch (start us, length us, event | category | flops | bytes accessed | tf_op | source)
XLA Modules:
  0.0 238.3 jit_solution(3313222832370976377)
XLA Ops:
  0.6 0.0 copy-start.2
  0.6 0.6 copy-done.2
  1.3 0.1 broadcast_in_dim.8
  1.4 0.7 broadcast_in_dim.9.gain
  2.1 230.6 %shard_map.111 = (bf16[384,256]{1,0:T(8,128)(2,1)}, bf16[32,2,32,128]{3,2,1,0:T(8,128)(2,1)}, bf16[32,2,32,128]{3,2,1,0:T(8,128)(2,1)}, bf16[32,2,32,128]{3,2,1,0:T(8,128)(2,1)}) custom-call(bf16[384,256]{1,0:T(8,128)(2,1)} %tok_hbm.1, f32[2,32,128]{2,1,0:T(8,128)} %broadcast_in_dim.9.gain, f32[32,2,32,128]{3,2,1,0:T(8,128)} %bitcast.9, ...), custom_call_target="tpu_custom_call" | custom-call | tf_op jit(solution)/shard_map/pallas_call | solution.py:307
  232.7 1.6 copy.16
  234.3 0.0 copy-start.1
  234.3 1.9 copy.17
  236.2 0.0 copy-done.1
  236.2 0.0 copy-start
  236.3 0.8 copy.18
  237.0 0.4 copy-done
  237.5 0.8 copy.19
Async XLA Ops:
  0.6 0.7 copy-start.2
  234.3 1.9 copy-start.1
  236.2 1.2 copy-start

commit v2 on v1

--- a/solution.py
+++ b/solution.py
@@ -15,8 +15,8 @@
 def kernel(
     cfg, tok_hbm, gain, gate_hbm, up_hbm, down_hbm, ids, glog, plog,
     mixed, gate_o, up_o, down_o,
-    wf, wstage, wbuf, wother, gu, dn, tokv, outs, trecv, piece, part, rsbuf, res, ret, onehot, cols,
-    lsem, osem, ws, wr, ts, tr, rs, rr, ys, yr, ds, dr, ags, agr, rss, rsr,
+    gains, wf, wstage, wbuf, wother, gu, dn, tokv, outs, trecv, piece, part, rsbuf, res, ret, onehot, cols,
+    ready, lsem, osem, ws, wr, ts, tr, rs, rr, ys, yr, ds, dr, ags, agr, rss, rsr,
 ):
     n, groups, tps, cap, slots, nq, ck = cfg
     half = n // 2
@@ -35,29 +35,41 @@
     tok_load.start()
 
     barrier = pltpu.get_barrier_semaphore()
-
-    def greet(axis, here, size):
-        def one(o, c):
-            pl.semaphore_signal(
-                barrier, inc=1, device_id={axis: lax.rem(here + o, size)}, device_id_type=MESH
-            )
+    rank = lax.rem(me + n - 1, n)
+
+    def loop(lo, hi, fn):
+        def one(i, c):
+            fn(i)
             return c
 
-        lax.fori_loop(1, size, one, 0)
-
-    greet("fs", me, n)
-    greet("tp", tp, tps)
-    greet("grp", grp, groups)
-
+        lax.fori_loop(lo, hi, one, 0)
+
+    def greet(axis, there):
+        pl.semaphore_signal(barrier, inc=1, device_id={axis: there}, device_id_type=MESH)
+
+    loop(1, n - rank, lambda i: greet("fs", lax.rem(me + i, n)))
+    loop(1, tps, lambda i: greet("tp", lax.rem(tp + i, tps)))
+    loop(1, groups, lambda i: greet("grp", lax.rem(grp + i, groups)))
+
+    rows = gain.shape[1]
+    diagonal = lax.broadcasted_iota(jnp.int32, (rows, rows), 0) == lax.broadcasted_iota(jnp.int32, (rows, rows), 1)
+    column = jnp.sum(jnp.where(diagonal, gain[...], 0.0), axis=1, keepdims=True)
+    gains[...] = jnp.broadcast_to(column, (rows, gains.shape[2])).reshape(gains.shape)
     for i, load in enumerate(loads):
         load.wait()
         if i < 2:
-            wstage[:, i] = (wf[i] * gain[grp][None]).astype(BF)
+            wstage[:, i] = (wf[i] * gains[grp][None]).astype(BF)
         else:
             wstage[:, i] = wf[i].astype(BF)
         wbuf[i, me, grp] = wstage[me, i]
 
-    pl.semaphore_wait(barrier, n - 1 + tps - 1 + groups - 1)
+    pl.semaphore_wait(barrier, rank + tps - 1 + groups - 1)
+
+    def report(i):
+        there = lax.rem(me + n - i, n)
+        pl.semaphore_signal(ready.at[i], inc=1, device_id={"fs": there}, device_id_type=MESH)
+
+    loop(1, rank + 1, report)
 
     def delta_of(h, k):
         return half - 1 - k if h == 0 else half + k
@@ -79,12 +91,18 @@
         if hi == half:
             fn(1, half - 1)
 
-    def w_copy(h, k, dst, src):
+    def w_copy(delta, dst, src):
         return pltpu.make_async_remote_copy(
             src_ref=wstage.at[dst], dst_ref=wbuf.at[:, src, grp],
-            send_sem=ws.at[h, k], recv_sem=wr.at[h, k],
+            send_sem=ws.at[delta], recv_sem=wr.at[delta],
             device_id={"fs": dst}, device_id_type=MESH,
         )
+
+    def w_to(delta):
+        return w_copy(delta, lax.rem(me + delta, n), me)
+
+    def w_from(delta):
+        return w_copy(delta, lax.rem(me + delta, n), lax.rem(me + n - delta, n))
 
     def t_copy(h, k, dst):
         return pltpu.make_async_remote_copy(
@@ -100,7 +118,7 @@
             device_id={"fs": dst}, device_id_type=MESH,
         )
 
-    every(lambda h, k: w_copy(h, k, to(h, k), me).start())
+    loop(1, rank + 1, lambda i: w_to(n - i).start())
 
     exp_group = n // glog.shape[0]
     first, second = ids[0:1, :], ids[1:2, :]
@@ -144,6 +162,11 @@
 
     lax.fori_loop(0, n // 4, fill, 0)
 
+    def late(i):
+        pl.semaphore_wait(ready.at[i], 1)
+        w_to(i).start()
+
+    loop(1, n - rank, late)
     every(lambda h, k: t_copy(h, k, to(h, k)).start())
     trecv[0, half - 1] = outs[me]
 
@@ -156,7 +179,7 @@
     for i in range(2):
         onehot[i] = (l_iota == cols[:, i : i + 1].astype(jnp.int32)).astype(F32).astype(BF)
 
-    every(lambda h, k: w_copy(h, k, to(h, k), back(h, k)).wait_recv())
+    loop(1, n, lambda delta: w_from(delta).wait_recv())
 
     def y_copy(o, there, whose):
         return pltpu.make_async_remote_copy(
@@ -204,11 +227,7 @@
         return lax.rem(tp + tps - o, tps)
 
     def around(fn):
-        def one(o, c):
-            fn(o)
-            return c
-
-        lax.fori_loop(1, tps, one, 0)
+        loop(1, tps, fn)
 
     def gather(q):
         every(lambda h, k: t_copy(h, k, to(h, k)).wait_recv(), q * ck, (q + 1) * ck)
@@ -274,7 +293,7 @@
 
     for store in stores:
         store.wait()
-    every(lambda h, k: w_copy(h, k, to(h, k), me).wait_send())
+    loop(1, n, lambda delta: w_to(delta).wait_send())
     every(lambda h, k: t_copy(h, k, to(h, k)).wait_send())
     every(lambda h, k: r_copy(h, k, back(h, k), me).wait_send())
     for o in range(1, groups):
@@ -283,6 +302,21 @@
     for q in range(nq):
         around(lambda o: ag_copy(q, o, ahead(o), tp).wait_send())
         around(lambda o: rs_copy(q, o, ahead(o), tp).wait_send())
+
+
+def hand_on(*refs):
+    count = (len(refs) - 2) // 3
+    given, taken, held = (refs[i * count : (i + 1) * count] for i in range(3))
+    isem, osem = refs[-2:]
+    loads = [pltpu.make_async_copy(a, b, isem.at[i]) for i, (a, b) in enumerate(zip(given, held))]
+    stores = [pltpu.make_async_copy(a, b, osem.at[i]) for i, (a, b) in enumerate(zip(held, taken))]
+    for load in loads:
+        load.start()
+    for load, store in zip(loads, stores):
+        load.wait()
+        store.start()
+    for store in stores:
+        store.wait()
 
 
 def body(chunks, tokens, norm_gain, gate_weight, up_weight, down_weight, ids, group_logits, pair_logits):
@@ -299,7 +333,7 @@
     def cut(weight):
         return weight.reshape(experts, groups, share, f)
 
-    gain = jnp.broadcast_to(norm_gain[:, None], (rows, f)).reshape(groups, share, f)
+    gain = norm_gain.reshape(1, rows)
     vmem = pl.BlockSpec(memory_space=pltpu.VMEM)
     hbm = pl.BlockSpec(memory_space=pl.ANY)
     whole = jax.ShapeDtypeStruct((n, groups, share, f), BF)
@@ -309,7 +343,9 @@
         out_shape=(jax.ShapeDtypeStruct((tok_rows, width), BF), whole, whole, whole),
         in_specs=[hbm, vmem, hbm, hbm, hbm, vmem, vmem, vmem],
         out_specs=(vmem, hbm, hbm, hbm),
+        name="experts",
         scratch_shapes=[
+            pltpu.VMEM((groups, share, f), F32),
             pltpu.VMEM((3, n, share, f), F32),
             pltpu.VMEM((n, 3, share, f), BF),
             pltpu.VMEM((3, n, groups, share, f), BF),
@@ -326,8 +362,8 @@
             pltpu.VMEM((n, slots, width), BF),
             pltpu.VMEM((2, tok_rows, n * slots), BF),
             pltpu.VMEM((tok_rows, 128), F32),
-            dma((4,)), dma((3,)),
-            dma((2, half)), dma((2, half)),
+            pltpu.SemaphoreType.REGULAR((n,)), dma((4,)), dma((3,)),
+            dma((n,)), dma((n,)),
             dma((2, half)), dma((2, half)),
             dma((2, half)), dma((2, half)),
             dma((groups,)), dma((groups,)),
@@ -340,7 +376,14 @@
         tokens, gain, cut(gate_weight), cut(up_weight), cut(down_weight),
         ids.T, group_logits.T, pair_logits.T,
     )
-    mixed, gate_out, up_out, down_out = out
+    shapes = [jax.ShapeDtypeStruct(a.shape, a.dtype) for a in out]
+    mixed, gate_out, up_out, down_out = pl.pallas_call(
+        hand_on,
+        out_shape=shapes,
+        in_specs=[hbm] * len(out),
+        out_specs=[hbm] * len(out),
+        scratch_shapes=[pltpu.VMEM(a.shape, a.dtype) for a in out] + [dma((len(out),)), dma((len(out),))],
+    )(*out)
     return (mixed,) + tuple(w.reshape(1, depth, f) for w in (gate_out, up_out, down_out))
 
 

time: 239 us -> 231 us (0.967)
  local copies, waits for them, and re-layouts: 6.99 us -> 0 us
    unnamed x10 -> x0, local copies, waits for them, and re-layouts: 6.22 us -> none
    pallas_call x1, Pallas kernels: 231 us -> 227 us  [body(): pl.pallas_call(functools.partial(kernel, (n, groups, tps, cap, slots, chu...]
where the time goes in v2:
time: 231 us; the launch traced here: 230 us
  Pallas kernels  230 us (100%)
    pallas_call x1, Pallas kernels, body(): pl.pallas_call(functools.partial(kernel, (n, groups, tps, cap, slots, chu...  227 us

profile of v2, /device:TPU:33, one launch (start us, length us, event | category | flops | bytes accessed | tf_op | source)
XLA Modules:
  0.0 230.3 jit_solution(1281570367920170192)
XLA Ops:
  0.6 227.3 %experts.1 = (bf16[384,256]{1,0:T(8,128)(2,1)}, bf16[32,2,32,128]{3,2,1,0:T(8,128)(2,1)}, bf16[32,2,32,128]{3,2,1,0:T(8,128)(2,1)}, bf16[32,2,32,128]{3,2,1,0:T(8,128)(2,1)}) custom-call(bf16[384,256]{1,0:T(8,128)(2,1)} %tok_hbm.1, f32[1,64]{1,0:T(1,128)} %bitcast.16, f32[32,2,32,128]{3,2,1,0:T(8,128)} %bitcast.10, f32[32,2,32,128]{3,2,1,0:T(8,128)} %bitcast.11, ...), custom_call_target="tpu_custom_call" | custom-call | tf_op jit(solution)/shard_map/experts/pallas_call | solution.py:341
  227.9 2.4 %shard_map.111 = (bf16[384,256]{1,0:T(8,128)(2,1)}, bf16[32,2,32,128]{3,2,1,0:T(8,128)(2,1)}, bf16[32,2,32,128]{3,2,1,0:T(8,128)(2,1)}, bf16[32,2,32,128]{3,2,1,0:T(8,128)(2,1)}) custom-call(bf16[384,256]{1,0:T(8,128)(2,1)} %get-tuple-element.12.refs_0_, bf16[32,2,32,128]{3,2,1,0:T(8,128)(2,1)} %get-tuple-element.13.refs_1_, ...), custom_call_target="tpu_custom_call" | custom-call | tf_op jit(solution)/shard_map/pallas_call | solution.py:380

commit v3 on v2

--- a/solution.py
+++ b/solution.py
@@ -15,10 +15,10 @@
 def kernel(
     cfg, tok_hbm, gain, gate_hbm, up_hbm, down_hbm, ids, glog, plog,
     mixed, gate_o, up_o, down_o,
-    gains, wf, wstage, wbuf, wother, gu, dn, tokv, outs, trecv, piece, part, rsbuf, res, ret, onehot, cols,
-    ready, lsem, osem, ws, wr, ts, tr, rs, rr, ys, yr, ds, dr, ags, agr, rss, rsr,
+    gains, wf, wstage, wbuf, wother, gu, dall, dn, tokv, outs, trecv, piece, hbuf, res, ret, onehot, cols,
+    ready, lsem, osem, ws, wr, ts, tr, rs, rr, ys, yr, ds, dr, ns, nr, ags, agr, hs, hr, es, er,
 ):
-    n, groups, tps, cap, slots, nq, ck = cfg
+    n, groups, tps, cap, slots, ck, order, plan = cfg
     half = n // 2
     tok_rows, width = tokv.shape
     me, grp, tp = lax.axis_index("fs"), lax.axis_index("grp"), lax.axis_index("tp")
@@ -111,9 +111,9 @@
             device_id={"fs": dst}, device_id_type=MESH,
         )
 
-    def r_copy(h, k, dst, src):
-        return pltpu.make_async_remote_copy(
-            src_ref=res.at[h, k], dst_ref=ret.at[src],
+    def r_copy(h, k, dst):
+        return pltpu.make_async_remote_copy(
+            src_ref=res.at[h, k], dst_ref=ret.at[h, k],
             send_sem=rs.at[h, k], recv_sem=rr.at[h, k],
             device_id={"fs": dst}, device_id_type=MESH,
         )
@@ -136,6 +136,13 @@
     slot0 = jnp.where(keep0, first.astype(F32) * slots + rank0, -1.0)
     slot1 = jnp.where(keep1, second.astype(F32) * slots + rank1, -1.0)
 
+    def place(expert, rank_in, keep):
+        rel = jnp.where(expert >= me, expert - me, expert - me + n)
+        spot = jnp.where(rel < half, half - 1 - rel, rel)
+        return jnp.where(keep, spot.astype(F32) * slots + rank_in, -1.0)
+
+    place0, place1 = place(first, rank0, keep0), place(second, rank1, keep1)
+
     group_exp = [jnp.exp(glog[g : g + 1, :]) for g in range(glog.shape[0])]
     chosen, total = jnp.zeros_like(slot0), jnp.zeros_like(slot0)
     for g, value in enumerate(group_exp):
@@ -167,37 +174,63 @@
         w_to(i).start()
 
     loop(1, n - rank, late)
-    every(lambda h, k: t_copy(h, k, to(h, k)).start())
+    for q in order:
+        every(lambda h, k: t_copy(h, k, to(h, k)).start(), q * ck, (q + 1) * ck)
     trecv[0, half - 1] = outs[me]
 
     lines = lax.broadcasted_iota(jnp.int32, (128, tok_rows), 0)
     packed = jnp.zeros((128, tok_rows), F32)
-    for i, row in enumerate((slot0, slot1, weight0, weight1)):
+    for i, row in enumerate((place0, place1, weight0, weight1)):
         packed = jnp.where(lines == i, row, packed)
     cols[...] = packed.T
     l_iota = lax.broadcasted_iota(jnp.int32, (tok_rows, n * slots), 1)
     for i in range(2):
         onehot[i] = (l_iota == cols[:, i : i + 1].astype(jnp.int32)).astype(F32).astype(BF)
 
-    loop(1, n, lambda delta: w_from(delta).wait_recv())
-
-    def y_copy(o, there, whose):
-        return pltpu.make_async_remote_copy(
-            src_ref=wbuf.at[:, :, grp], dst_ref=wbuf.at[:, :, whose],
-            send_sem=ys.at[o], recv_sem=yr.at[o],
-            device_id={"grp": there}, device_id_type=MESH,
-        )
-
-    for o in range(1, groups):
-        y_copy(o, lax.rem(grp + o, groups), grp).start()
-    for o in range(1, groups):
-        y_copy(o, lax.rem(grp + o, groups), lax.rem(grp + groups - o, groups)).wait_recv()
-
-    exchange = pltpu.make_async_remote_copy(
-        src_ref=wbuf, dst_ref=wother, send_sem=ds, recv_sem=dr,
-        device_id={"tp": partner}, device_id_type=MESH,
-    )
-    exchange.start()
+    def delta_at(p):
+        return jnp.where(lax.rem(p, 2) == 1, (p + 1) // 2, lax.rem(n - p // 2, n))
+
+    def source_at(p):
+        return lax.rem(me + n - delta_at(p), n)
+
+    batch = n // yr.shape[1]
+
+    def y_copy(o, p):
+        spot = wbuf.at[:, source_at(p), grp]
+        return pltpu.make_async_remote_copy(
+            src_ref=spot, dst_ref=spot, send_sem=ys.at[o], recv_sem=yr.at[o, p // batch],
+            device_id={"grp": lax.rem(grp + o, groups)}, device_id_type=MESH,
+        )
+
+    def d_copy(p, whose):
+        at = source_at(p)
+        return pltpu.make_async_remote_copy(
+            src_ref=wbuf.at[0:2, at, whose], dst_ref=wother.at[:, at, whose], send_sem=ds, recv_sem=dr,
+            device_id={"tp": partner}, device_id_type=MESH,
+        )
+
+    def pass_on(p):
+        loop(1, groups, lambda o: y_copy(o, p).start())
+        d_copy(p, grp).start()
+
+    def landed(p):
+        w_from(delta_at(p)).wait_recv()
+        pass_on(p)
+
+    pass_on(0)
+    loop(1, n, landed)
+
+    def shared(o):
+        whose = lax.rem(grp + groups - o, groups)
+
+        def some(b):
+            blocks = wbuf.at[:, pl.ds(0, batch), 0]
+            pltpu.make_async_copy(blocks, blocks, yr.at[o, b]).wait()
+            loop(b * batch, (b + 1) * batch, lambda p: d_copy(p, whose).start())
+
+        loop(0, n // batch, some)
+
+    loop(1, groups, shared)
     stores = [
         pltpu.make_async_copy(wbuf.at[i], dst, osem.at[i])
         for i, dst in enumerate((gate_o, up_o, down_o))
@@ -213,11 +246,38 @@
             device_id={"tp": there}, device_id_type=MESH,
         )
 
-    def rs_copy(q, o, there, whose):
-        return pltpu.make_async_remote_copy(
-            src_ref=part.at[q, there], dst_ref=rsbuf.at[q, whose],
-            send_sem=rss.at[q, o], recv_sem=rsr.at[q, o],
+    dn_src = dall.shape[1]
+
+    def n_copy(o, there, whose):
+        return pltpu.make_async_remote_copy(
+            src_ref=wbuf.at[2, pl.ds(there * dn_src, dn_src)], dst_ref=dall.at[whose],
+            send_sem=ns.at[o], recv_sem=nr.at[o],
             device_id={"tp": there}, device_id_type=MESH,
+        )
+
+    f = wbuf.shape[-1]
+    chip = tp // 2
+    chips = tps // 2
+
+    def h_copy(q, o):
+        spot = hbuf.at[q, chip, core]
+        return pltpu.make_async_remote_copy(
+            src_ref=spot, dst_ref=spot, send_sem=hs.at[q, o], recv_sem=hr.at[q, o],
+            device_id={"tp": lax.rem(tp + 2 * o, tps)}, device_id_type=MESH,
+        )
+
+    def h_from(q, o):
+        spot = hbuf.at[q, lax.rem(chip + chips - o, chips), core]
+        return pltpu.make_async_remote_copy(
+            src_ref=spot, dst_ref=spot, send_sem=hs.at[q, o], recv_sem=hr.at[q, o],
+            device_id={"tp": lax.rem(tp + 2 * o, tps)}, device_id_type=MESH,
+        )
+
+    def e_copy(q, o, side):
+        spot = hbuf.at[q, lax.rem(chip + chips - o, chips), side]
+        return pltpu.make_async_remote_copy(
+            src_ref=spot, dst_ref=spot, send_sem=es.at[q, o], recv_sem=er.at[q, o],
+            device_id={"tp": partner}, device_id_type=MESH,
         )
 
     def ahead(o):
@@ -232,76 +292,113 @@
     def gather(q):
         every(lambda h, k: t_copy(h, k, to(h, k)).wait_recv(), q * ck, (q + 1) * ck)
         around(lambda o: ag_copy(q, o, ahead(o), tp).start())
-        piece[q, tp] = trecv[core, q * ck : (q + 1) * ck]
+
+    def block(j):
+        return pl.ds(pl.multiple_of(j * width, width), width)
 
     def work(q):
-        around(lambda o: ag_copy(q, o, ahead(o), behind(o)).wait_recv())
         rows = ck * slots
-        acc = jnp.zeros((rows, gu.shape[1]), F32)
-        for j in range(tps):
+        acc = jnp.dot(
+            trecv[core, q * ck : (q + 1) * ck].reshape(rows, width), gu[block(tp), :],
+            preferred_element_type=F32,
+        )
+        for o in range(1, tps):
+            j = behind(o)
+            ag_copy(q, o, ahead(o), j).wait_recv()
             acc += jnp.dot(
-                piece[q, j].reshape(rows, width), gu[j * width : (j + 1) * width, :],
-                preferred_element_type=F32,
+                piece[q, j].reshape(rows, width), gu[block(j), :], preferred_element_type=F32
             )
         f = gu.shape[1] // 4
         hidden = []
         for i in range(2):
             gate_v, up_v = acc[:, 2 * i * f : (2 * i + 1) * f], acc[:, (2 * i + 1) * f : (2 * i + 2) * f]
-            hidden.append((gate_v / (1.0 + jnp.exp(-gate_v)) * up_v).astype(BF))
-        hidden = jnp.concatenate(hidden, axis=1)
-        for j in range(tps):
-            term = lax.dot_general(
-                hidden, dn[j * width : (j + 1) * width, :], (((1,), (1,)), ((), ())),
-                preferred_element_type=F32,
-            )
-            part[q, j] = term.astype(BF).reshape(ck, slots, width)
-        around(lambda o: rs_copy(q, o, ahead(o), tp).start())
-        rsbuf[q, tp] = part[q, tp]
+            hidden.append(gate_v / (1.0 + jnp.exp(-gate_v)) * up_v)
+        low = jnp.where(core == 0, hidden[0], hidden[1])
+        high = jnp.where(core == 0, hidden[1], hidden[0])
+        hbuf[q, chip, core, :, 0:f] = low.astype(BF)
+        hbuf[q, chip, core, :, f : 2 * f] = high.astype(BF)
+        for o in range(1, chips):
+            h_copy(q, o).start()
+        e_copy(q, 0, core).start()
+
+    def relay(q):
+        for o in range(1, chips):
+            h_from(q, o).wait_recv()
+            e_copy(q, o, core).start()
+
+    def join_down():
+        around(lambda o: n_copy(o, ahead(o), behind(o)).wait_recv())
+        for x in range(chips):
+            for i in range(2):
+                dn[x, :, i * f : (i + 1) * f] = dall[2 * x + i].reshape(width, f)
 
     def finish(q):
-        around(lambda o: rs_copy(q, o, ahead(o), behind(o)).wait_recv())
+        for o in range(chips):
+            e_copy(q, o, 1 - core).wait_recv()
         for h in range(2):
-            total = rsbuf[q, h].astype(F32)
-            for chip in range(1, tps // 2):
-                total += rsbuf[q, 2 * chip + h].astype(F32)
-            res[h, q * ck : (q + 1) * ck] = total.astype(BF)
-        every(lambda h, k: r_copy(h, k, back(h, k), me).start(), q * ck, (q + 1) * ck)
-
-    gather(0)
-    exchange.wait_recv()
-    f = wbuf.shape[-1]
+            total = jnp.zeros((ck * slots, width), F32)
+            for x in range(chips):
+                total += lax.dot_general(
+                    hbuf[q, x, h], dn[x], (((1,), (1,)), ((), ())), preferred_element_type=F32
+                )
+            res[h, q * ck : (q + 1) * ck] = total.astype(BF).reshape(ck, slots, width)
+        every(lambda h, k: r_copy(h, k, back(h, k)).start(), q * ck, (q + 1) * ck)
+
+    around(lambda o: n_copy(o, ahead(o), tp).start())
+    dall[tp] = wbuf[2, pl.ds(tp * dn_src, dn_src)]
+    gather(order[0])
+    pltpu.make_async_copy(wother, wother, dr).wait()
     depth = gu.shape[0]
     for i, src in enumerate((wbuf, wother)):
         gu[:, 2 * i * f : (2 * i + 1) * f] = src[0].reshape(depth, f)
         gu[:, (2 * i + 1) * f : (2 * i + 2) * f] = src[1].reshape(depth, f)
-        dn[:, i * f : (i + 1) * f] = src[2].reshape(depth, f)
-
-    todo = []
-    for q in range(nq):
-        todo += [(2 * q + 0.0, gather, q), (2 * q + 1.1, work, q), (2 * q + 3.2, finish, q)]
-    for _, step, q in sorted(todo, key=lambda item: item[0])[1:]:
-        step(q)
-
-    ret[me] = res[0, half - 1]
-    every(lambda h, k: r_copy(h, k, back(h, k), to(h, k)).wait_recv())
-    table = ret[...].reshape(n * slots, width)
+
+    steps = [gather, work, relay, finish]
+    for at, step in plan:
+        if (at, step) == (0, FINISH):
+            join_down()
+        steps[step](order[at])
+
+    ret[0, half - 1] = res[0, half - 1]
     mix = jnp.zeros((tok_rows, width), F32)
-    for i in range(2):
-        rows = jnp.dot(onehot[i], table, preferred_element_type=F32)
-        mix += rows * cols[:, 2 + i : 3 + i]
+    for q in order:
+        every(lambda h, k: r_copy(h, k, back(h, k)).wait_recv(), q * ck, (q + 1) * ck)
+        for h in range(2):
+            table = ret[h, q * ck : (q + 1) * ck].reshape(ck * slots, width)
+            start = (h * half + q * ck) * slots
+            for i in range(2):
+                rows = jnp.dot(
+                    onehot[i, :, start : start + ck * slots], table, preferred_element_type=F32
+                )
+                mix += rows * cols[:, 2 + i : 3 + i]
     mixed[...] = mix.astype(BF)
 
     for store in stores:
         store.wait()
     loop(1, n, lambda delta: w_to(delta).wait_send())
     every(lambda h, k: t_copy(h, k, to(h, k)).wait_send())
-    every(lambda h, k: r_copy(h, k, back(h, k), me).wait_send())
-    for o in range(1, groups):
-        y_copy(o, lax.rem(grp + o, groups), grp).wait_send()
-    exchange.wait_send()
-    for q in range(nq):
+    every(lambda h, k: r_copy(h, k, back(h, k)).wait_send())
+    mine = wbuf.at[:, :, grp]
+    loop(1, groups, lambda o: pltpu.make_async_copy(mine, mine, ys.at[o]).wait())
+    pltpu.make_async_copy(wother, wother, ds).wait()
+    around(lambda o: n_copy(o, ahead(o), tp).wait_send())
+    for q in order:
         around(lambda o: ag_copy(q, o, ahead(o), tp).wait_send())
-        around(lambda o: rs_copy(q, o, ahead(o), tp).wait_send())
+        for o in range(chips):
+            if o:
+                h_copy(q, o).wait_send()
+            e_copy(q, o, core).wait_send()
+
+
+GATHER, WORK, RELAY, FINISH = range(4)
+
+
+def plan_of(chunks):
+    plan = []
+    for q in range(chunks):
+        plan += [(q, GATHER), (q - 1, RELAY), (q - 1, FINISH), (q, WORK)] if q else [(0, WORK)]
+    plan += [(chunks - 1, RELAY), (chunks - 1, FINISH)]
+    return tuple(plan)
 
 
 def hand_on(*refs):
@@ -319,13 +416,14 @@
         store.wait()
 
 
-def body(chunks, tokens, norm_gain, gate_weight, up_weight, down_weight, ids, group_logits, pair_logits):
+def body(order, tokens, norm_gain, gate_weight, up_weight, down_weight, ids, group_logits, pair_logits):
     experts, rows, f = gate_weight.shape
     tok_rows, width = tokens.shape
     n, groups, tps = lax.axis_size("fs"), lax.axis_size("grp"), lax.axis_size("tp")
     cap = 5 * tok_rows * 2 // (4 * experts)
     slots = -(-cap // 16) * 16
     half = n // 2
+    chunks = len(order)
     ck = half // chunks
     share = rows // groups
     depth = n * rows
@@ -339,7 +437,7 @@
     whole = jax.ShapeDtypeStruct((n, groups, share, f), BF)
     dma = pltpu.SemaphoreType.DMA
     out = pl.pallas_call(
-        functools.partial(kernel, (n, groups, tps, cap, slots, chunks, ck)),
+        functools.partial(kernel, (n, groups, tps, cap, slots, ck, order, plan_of(chunks))),
         out_shape=(jax.ShapeDtypeStruct((tok_rows, width), BF), whole, whole, whole),
         in_specs=[hbm, vmem, hbm, hbm, hbm, vmem, vmem, vmem],
         out_specs=(vmem, hbm, hbm, hbm),
@@ -349,27 +447,29 @@
             pltpu.VMEM((3, n, share, f), F32),
             pltpu.VMEM((n, 3, share, f), BF),
             pltpu.VMEM((3, n, groups, share, f), BF),
-            pltpu.VMEM((3, n, groups, share, f), BF),
+            pltpu.VMEM((2, n, groups, share, f), BF),
             pltpu.VMEM((depth, 4 * f), BF),
-            pltpu.VMEM((depth, 2 * f), BF),
+            pltpu.VMEM((tps, n // tps, groups, share, f), BF),
+            pltpu.VMEM((tps // 2, width, 2 * f), BF),
             pltpu.VMEM((tok_rows, width), BF),
             pltpu.VMEM((n, slots, width), BF),
             pltpu.VMEM((2, half, slots, width), BF),
             pltpu.VMEM((chunks, tps, ck, slots, width), BF),
-            pltpu.VMEM((chunks, tps, ck, slots, width), BF),
-            pltpu.VMEM((chunks, tps, ck, slots, width), BF),
+            pltpu.VMEM((chunks, tps // 2, 2, ck * slots, 2 * f), BF),
             pltpu.VMEM((2, half, slots, width), BF),
-            pltpu.VMEM((n, slots, width), BF),
+            pltpu.VMEM((2, half, slots, width), BF),
             pltpu.VMEM((2, tok_rows, n * slots), BF),
             pltpu.VMEM((tok_rows, 128), F32),
             pltpu.SemaphoreType.REGULAR((n,)), dma((4,)), dma((3,)),
             dma((n,)), dma((n,)),
             dma((2, half)), dma((2, half)),
             dma((2, half)), dma((2, half)),
-            dma((groups,)), dma((groups,)),
+            dma((groups,)), dma((groups, 4)),
             dma, dma,
+            dma((tps,)), dma((tps,)),
             dma((chunks, tps)), dma((chunks, tps)),
-            dma((chunks, tps)), dma((chunks, tps)),
+            dma((chunks, tps // 2)), dma((chunks, tps // 2)),
+            dma((chunks, tps // 2)), dma((chunks, tps // 2)),
         ],
         compiler_params=pltpu.CompilerParams(collective_id=0, has_side_effects=True),
     )(
@@ -387,7 +487,7 @@
     return (mixed,) + tuple(w.reshape(1, depth, f) for w in (gate_out, up_out, down_out))
 
 
-def solution(mesh, chunks=4):
+def solution(mesh, order=(0, 1, 2, 3)):
     placed = (
         P(("grp", "fs"), "tp"),
         P("fs"),
@@ -399,7 +499,7 @@
         P(("grp", "fs"), None),
     )
     return jax.shard_map(
-        functools.partial(body, chunks),
+        functools.partial(body, order),
         mesh=mesh,
         in_specs=placed,
         out_specs=(

time: 231 us -> 221 us (0.957)
  Pallas kernels: 230 us -> 219 us
    pallas_call x1, Pallas kernels: 227 us -> 217 us  [body(): pl.pallas_call(functools.partial(kernel, (n, groups, tps, cap, slots, ck,...]
where the time goes in v3:
time: 221 us; the launch traced here: 220 us
  Pallas kernels  219 us (99%)
    pallas_call x1, Pallas kernels, body(): pl.pallas_call(functools.partial(kernel, (n, groups, tps, cap, slots, ck,...  217 us

profile of v3, /device:TPU:33, one launch (start us, length us, event | category | flops | bytes accessed | tf_op | source)
XLA Modules:
  0.0 219.8 jit_solution(16363465096680321730)
XLA Ops:
  0.6 216.8 %experts.1 = (bf16[384,256]{1,0:T(8,128)(2,1)}, bf16[32,2,32,128]{3,2,1,0:T(8,128)(2,1)}, bf16[32,2,32,128]{3,2,1,0:T(8,128)(2,1)}, bf16[32,2,32,128]{3,2,1,0:T(8,128)(2,1)}) custom-call(bf16[384,256]{1,0:T(8,128)(2,1)} %tok_hbm.1, f32[1,64]{1,0:T(1,128)} %bitcast.16, f32[32,2,32,128]{3,2,1,0:T(8,128)} %bitcast.10, f32[32,2,32,128]{3,2,1,0:T(8,128)} %bitcast.11, ...), custom_call_target="tpu_custom_call" | custom-call | tf_op jit(solution)/shard_map/experts/pallas_call | solution.py:439
  217.5 2.4 %shard_map.111 = (bf16[384,256]{1,0:T(8,128)(2,1)}, bf16[32,2,32,128]{3,2,1,0:T(8,128)(2,1)}, bf16[32,2,32,128]{3,2,1,0:T(8,128)(2,1)}, bf16[32,2,32,128]{3,2,1,0:T(8,128)(2,1)}) custom-call(bf16[384,256]{1,0:T(8,128)(2,1)} %get-tuple-element.12.refs_0_, bf16[32,2,32,128]{3,2,1,0:T(8,128)(2,1)} %get-tuple-element.13.refs_1_, ...), custom_call_target="tpu_custom_call" | custom-call | tf_op jit(solution)/shard_map/pallas_call | solution.py:480

commit v4 on v3

--- a/solution.py
+++ b/solution.py
@@ -217,6 +217,61 @@
         w_from(delta_at(p)).wait_recv()
         pass_on(p)
 
+    def ag_copy(q, o, there, whose):
+        h = lax.rem(there, 2)
+        return pltpu.make_async_remote_copy(
+            src_ref=trecv.at[h, pl.ds(q * ck, ck)], dst_ref=piece.at[q, whose],
+            send_sem=ags.at[q, o], recv_sem=agr.at[q, o],
+            device_id={"tp": there}, device_id_type=MESH,
+        )
+
+    dn_src = dall.shape[1]
+
+    def n_copy(o, there, whose):
+        return pltpu.make_async_remote_copy(
+            src_ref=wbuf.at[2, pl.ds(there * dn_src, dn_src)], dst_ref=dall.at[whose],
+            send_sem=ns.at[o], recv_sem=nr.at[o],
+            device_id={"tp": there}, device_id_type=MESH,
+        )
+
+    f = wbuf.shape[-1]
+    chip = tp // 2
+    chips = tps // 2
+
+    def h_copy(q, o):
+        spot = hbuf.at[q, chip, core]
+        return pltpu.make_async_remote_copy(
+            src_ref=spot, dst_ref=spot, send_sem=hs.at[q, o], recv_sem=hr.at[q, o],
+            device_id={"tp": lax.rem(tp + 2 * o, tps)}, device_id_type=MESH,
+        )
+
+    def h_from(q, o):
+        spot = hbuf.at[q, lax.rem(chip + chips - o, chips), core]
+        return pltpu.make_async_remote_copy(
+            src_ref=spot, dst_ref=spot, send_sem=hs.at[q, o], recv_sem=hr.at[q, o],
+            device_id={"tp": lax.rem(tp + 2 * o, tps)}, device_id_type=MESH,
+        )
+
+    def e_copy(q, o, side):
+        spot = hbuf.at[q, lax.rem(chip + chips - o, chips), side]
+        return pltpu.make_async_remote_copy(
+            src_ref=spot, dst_ref=spot, send_sem=es.at[q, o], recv_sem=er.at[q, o],
+            device_id={"tp": partner}, device_id_type=MESH,
+        )
+
+    def ahead(o):
+        return lax.rem(tp + o, tps)
+
+    def behind(o):
+        return lax.rem(tp + tps - o, tps)
+
+    def around(fn):
+        loop(1, tps, fn)
+
+    def gather(q):
+        every(lambda h, k: t_copy(h, k, to(h, k)).wait_recv(), q * ck, (q + 1) * ck)
+        around(lambda o: ag_copy(q, o, ahead(o), tp).start())
+
     pass_on(0)
     loop(1, n, landed)
 
@@ -231,67 +286,13 @@
         loop(0, n // batch, some)
 
     loop(1, groups, shared)
+    gather(order[0])
     stores = [
         pltpu.make_async_copy(wbuf.at[i], dst, osem.at[i])
         for i, dst in enumerate((gate_o, up_o, down_o))
     ]
     for store in stores:
         store.start()
-
-    def ag_copy(q, o, there, whose):
-        h = lax.rem(there, 2)
-        return pltpu.make_async_remote_copy(
-            src_ref=trecv.at[h, pl.ds(q * ck, ck)], dst_ref=piece.at[q, whose],
-            send_sem=ags.at[q, o], recv_sem=agr.at[q, o],
-            device_id={"tp": there}, device_id_type=MESH,
-        )
-
-    dn_src = dall.shape[1]
-
-    def n_copy(o, there, whose):
-        return pltpu.make_async_remote_copy(
-            src_ref=wbuf.at[2, pl.ds(there * dn_src, dn_src)], dst_ref=dall.at[whose],
-            send_sem=ns.at[o], recv_sem=nr.at[o],
-            device_id={"tp": there}, device_id_type=MESH,
-        )
-
-    f = wbuf.shape[-1]
-    chip = tp // 2
-    chips = tps // 2
-
-    def h_copy(q, o):
-        spot = hbuf.at[q, chip, core]
-        return pltpu.make_async_remote_copy(
-            src_ref=spot, dst_ref=spot, send_sem=hs.at[q, o], recv_sem=hr.at[q, o],
-            device_id={"tp": lax.rem(tp + 2 * o, tps)}, device_id_type=MESH,
-        )
-
-    def h_from(q, o):
-        spot = hbuf.at[q, lax.rem(chip + chips - o, chips), core]
-        return pltpu.make_async_remote_copy(
-            src_ref=spot, dst_ref=spot, send_sem=hs.at[q, o], recv_sem=hr.at[q, o],
-            device_id={"tp": lax.rem(tp + 2 * o, tps)}, device_id_type=MESH,
-        )
-
-    def e_copy(q, o, side):
-        spot = hbuf.at[q, lax.rem(chip + chips - o, chips), side]
-        return pltpu.make_async_remote_copy(
-            src_ref=spot, dst_ref=spot, send_sem=es.at[q, o], recv_sem=er.at[q, o],
-            device_id={"tp": partner}, device_id_type=MESH,
-        )
-
-    def ahead(o):
-        return lax.rem(tp + o, tps)
-
-    def behind(o):
-        return lax.rem(tp + tps - o, tps)
-
-    def around(fn):
-        loop(1, tps, fn)
-
-    def gather(q):
-        every(lambda h, k: t_copy(h, k, to(h, k)).wait_recv(), q * ck, (q + 1) * ck)
-        around(lambda o: ag_copy(q, o, ahead(o), tp).start())
 
     def block(j):
         return pl.ds(pl.multiple_of(j * width, width), width)
@@ -332,21 +333,29 @@
             for i in range(2):
                 dn[x, :, i * f : (i + 1) * f] = dall[2 * x + i].reshape(width, f)
 
+    def side(q, h):
+        lo, hi = q * ck, (q + 1) * ck
+        total = jnp.zeros((ck * slots, width), F32)
+        for x in range(chips):
+            total += lax.dot_general(
+                hbuf[q, x, h], dn[x], (((1,), (1,)), ((), ())), preferred_element_type=F32
+            )
+        res[h, lo:hi] = total.astype(BF).reshape(ck, slots, width)
+
+        def send(k):
+            delta = jnp.where(h == 0, half - 1 - k, half + k)
+            r_copy(h, k, lax.rem(me + n - delta, n)).start()
+
+        loop(lo, hi - jnp.where(h == 0, 1, 0) if hi == half else hi, send)
+
     def finish(q):
+        side(q, core)
         for o in range(chips):
             e_copy(q, o, 1 - core).wait_recv()
-        for h in range(2):
-            total = jnp.zeros((ck * slots, width), F32)
-            for x in range(chips):
-                total += lax.dot_general(
-                    hbuf[q, x, h], dn[x], (((1,), (1,)), ((), ())), preferred_element_type=F32
-                )
-            res[h, q * ck : (q + 1) * ck] = total.astype(BF).reshape(ck, slots, width)
-        every(lambda h, k: r_copy(h, k, back(h, k)).start(), q * ck, (q + 1) * ck)
+        side(q, 1 - core)
 
     around(lambda o: n_copy(o, ahead(o), tp).start())
     dall[tp] = wbuf[2, pl.ds(tp * dn_src, dn_src)]
-    gather(order[0])
     pltpu.make_async_copy(wother, wother, dr).wait()
     depth = gu.shape[0]
     for i, src in enumerate((wbuf, wother)):
@@ -360,24 +369,10 @@
         steps[step](order[at])
 
     ret[0, half - 1] = res[0, half - 1]
-    mix = jnp.zeros((tok_rows, width), F32)
-    for q in order:
-        every(lambda h, k: r_copy(h, k, back(h, k)).wait_recv(), q * ck, (q + 1) * ck)
-        for h in range(2):
-            table = ret[h, q * ck : (q + 1) * ck].reshape(ck * slots, width)
-            start = (h * half + q * ck) * slots
-            for i in range(2):
-                rows = jnp.dot(
-                    onehot[i, :, start : start + ck * slots], table, preferred_element_type=F32
-                )
-                mix += rows * cols[:, 2 + i : 3 + i]
-    mixed[...] = mix.astype(BF)
-
     for store in stores:
         store.wait()
     loop(1, n, lambda delta: w_to(delta).wait_send())
     every(lambda h, k: t_copy(h, k, to(h, k)).wait_send())
-    every(lambda h, k: r_copy(h, k, back(h, k)).wait_send())
     mine = wbuf.at[:, :, grp]
     loop(1, groups, lambda o: pltpu.make_async_copy(mine, mine, ys.at[o]).wait())
     pltpu.make_async_copy(wother, wother, ds).wait()
@@ -388,6 +383,18 @@
             if o:
                 h_copy(q, o).wait_send()
             e_copy(q, o, core).wait_send()
+    mix = jnp.zeros((tok_rows, width), F32)
+    for q in order:
+        every(lambda h, k: r_copy(h, k, back(h, k)).wait(), q * ck, (q + 1) * ck)
+        for h in range(2):
+            table = ret[h, q * ck : (q + 1) * ck].reshape(ck * slots, width)
+            start = (h * half + q * ck) * slots
+            for i in range(2):
+                rows = jnp.dot(
+                    onehot[i, :, start : start + ck * slots], table, preferred_element_type=F32
+                )
+                mix += rows * cols[:, 2 + i : 3 + i]
+    mixed[...] = mix.astype(BF)
 
 
 GATHER, WORK, RELAY, FINISH = range(4)

time: 221 us -> 220 us (level)
  Pallas kernels: 219 us -> 216 us
    pallas_call x1, Pallas kernels: 217 us -> 214 us  [body(): pl.pallas_call(functools.partial(kernel, (n, groups, tps, cap, slots, ck,...]
where the time goes in v4:
time: 220 us; the launch traced here: 217 us
  Pallas kernels  216 us (98%)
    pallas_call x1, Pallas kernels, body(): pl.pallas_call(functools.partial(kernel, (n, groups, tps, cap, slots, ck,...  214 us

profile of v4, /device:TPU:33, one launch (start us, length us, event | category | flops | bytes accessed | tf_op | source)
XLA Modules:
  0.0 216.9 jit_solution(10238480287110237)
XLA Ops:
  0.6 213.9 %experts.1 = (bf16[384,256]{1,0:T(8,128)(2,1)}, bf16[32,2,32,128]{3,2,1,0:T(8,128)(2,1)}, bf16[32,2,32,128]{3,2,1,0:T(8,128)(2,1)}, bf16[32,2,32,128]{3,2,1,0:T(8,128)(2,1)}) custom-call(bf16[384,256]{1,0:T(8,128)(2,1)} %tok_hbm.1, f32[1,64]{1,0:T(1,128)} %bitcast.16, f32[32,2,32,128]{3,2,1,0:T(8,128)} %bitcast.10, f32[32,2,32,128]{3,2,1,0:T(8,128)} %bitcast.11, ...), custom_call_target="tpu_custom_call" | custom-call | tf_op jit(solution)/shard_map/experts/pallas_call | solution.py:446
  214.5 2.4 %shard_map.111 = (bf16[384,256]{1,0:T(8,128)(2,1)}, bf16[32,2,32,128]{3,2,1,0:T(8,128)(2,1)}, bf16[32,2,32,128]{3,2,1,0:T(8,128)(2,1)}, bf16[32,2,32,128]{3,2,1,0:T(8,128)(2,1)}) custom-call(bf16[384,256]{1,0:T(8,128)(2,1)} %get-tuple-element.12.refs_0_, bf16[32,2,32,128]{3,2,1,0:T(8,128)(2,1)} %get-tuple-element.13.refs_1_, ...), custom_call_target="tpu_custom_call" | custom-call | tf_op jit(solution)/shard_map/pallas_call | solution.py:487
